TPU v7x, 256 devices: a whole 4x4x8 slice. The times are simulated.
256 devices in a mesh: row: 32 (over z, x), col: 8 (over y, core).
Axes of the slice: x: 4, y: 4, z: 8, core: 2. Of those that a mesh axis runs over, the one named last changes fastest.
Arguments:
- tokens: bfloat16 [8192, 2048], P('row'), may hold values from -6 to 6
- norm_gain: float32 [2048], replicated, may hold values from 0.5 to 1.5
- first_gate: bfloat16 [2048, 1024], P(None, 'col'), may hold values from -0.125 to 0.125
- second_gate: bfloat16 [2048, 1024], P(None, 'col'), may hold values from -0.125 to 0.125
- value_weight: bfloat16 [2048, 1024], P(None, 'col'), may hold values from -0.125 to 0.125
- short_weight: bfloat16 [3, 3, 1024], P(None, None, 'col'), may hold values from -3.5 to 3.5
- short_bias: float32 [3, 1024], P(None, 'col'), may hold values from -2 to 2
- embed_weight: float32 [33, 64], replicated, may hold values from -1 to 1
- embed_bias: float32 [64], replicated, may hold values from -3 to 3
- inner_weight: float32 [64, 64], replicated, may hold values from -0.75 to 0.75
- inner_bias: float32 [64], replicated, may hold values from -3 to 3
- filter_freq: float32 [64], replicated, may hold values from 0.5 to 1.5
- filter_weight: float32 [2, 2, 64, 1024], P(None, None, None, ('col', 'row')), may hold values from -0.0234375 to 0.0234375
- filter_skip: float32 [2, 1024], P(None, ('col', 'row')), may hold values from -3 to 3
- output_gain: float32 [1024], P('col'), may hold values from 0.5 to 1.5
- output_weight: bfloat16 [1024, 2048], replicated, may hold values from -0.1875 to 0.1875
Outputs:
- mixed_output: bfloat16 [8192, 2048], P(('row', 'col'))
All inputs are finite; a program needn't handle non-finite values.
Results may differ from a plain program's by a relative error of at most 0.01.
Values may be sent and summed in bfloat16 or wider, within the bound.
A program may use at most 64 MiB of HBM per device.

v0:
```python
import functools
import math

import jax
import jax.numpy as jnp
import numpy as np
from jax import lax
from jax.experimental import pallas as pl
from jax.experimental.pallas import tpu as pltpu
from jax.sharding import PartitionSpec as P

CHANNELS = 1024
GROUPS = 8
FREQ_BANDS = 16


HIGHEST = lax.Precision.HIGHEST
NORM_EPS = 1e-06
DECAY_TARGET = 0.01
FAST_SPAN = 0.3
SLOW_SPAN = 1.5


def for_sending(value):
    return jax.tree.map(lambda a: a.astype(jnp.bfloat16) if a.dtype == jnp.float32 else a, value)


def position_features(length):
    position_ramp = jnp.linspace(0.0, 1.0, length, dtype=jnp.float32)[:, None]
    angles = 2.0 * math.pi * jnp.arange(length, dtype=jnp.float32)[:, None] / length
    band_freqs = jnp.linspace(0.0001, FREQ_BANDS - 1, FREQ_BANDS, dtype=jnp.float32)[None, :]
    features = jnp.concatenate(
        [position_ramp, jnp.cos(band_freqs * angles), -jnp.sin(band_freqs * angles)], axis=1
    )
    return (position_ramp, features)


def filter_hidden(length, embed_weight, embed_bias, inner_weight, inner_bias, filter_freq):
    position_ramp, features = position_features(length)
    hidden = jnp.sin(
        filter_freq * (jnp.dot(features, embed_weight, precision=HIGHEST) + embed_bias)
    )
    hidden = jnp.sin(filter_freq * (jnp.dot(hidden, inner_weight, precision=HIGHEST) + inner_bias))
    return (position_ramp, hidden)


def decay_rates():
    fastest = math.log(DECAY_TARGET) / FAST_SPAN
    slowest = math.log(DECAY_TARGET) / SLOW_SPAN
    return jnp.abs(jnp.linspace(slowest, fastest, CHANNELS, dtype=jnp.float32))


def short_filter(padded, weights, bias_row, length):
    result = bias_row.astype(jnp.float32)
    for tap_index in range(weights.shape[0]):
        result = result + padded[tap_index : tap_index + length].astype(jnp.float32) * weights[
            tap_index
        ].astype(jnp.float32)
    return result


def phase_table(rows, cols, period):
    phase_index = (
        lax.broadcasted_iota(jnp.int32, (rows, cols), 0)
        * lax.broadcasted_iota(jnp.int32, (rows, cols), 1)
        % period
    )
    phase_angle = phase_index.astype(jnp.float32) * (2.0 * math.pi / period)
    return (jnp.cos(phase_angle), jnp.sin(phase_angle))


def split_length(total_size):
    chosen = 2
    for candidate in range(2, math.isqrt(total_size) + 1, 2):
        if total_size % candidate == 0:
            chosen = candidate
    return chosen


def make_tables(total_size):
    major_size = split_length(total_size)
    minor_size = total_size // major_size
    inner_table = phase_table(major_size, major_size, major_size)
    twiddle = phase_table(major_size, minor_size, total_size)
    outer_table = phase_table(minor_size, minor_size, minor_size)
    return (major_size, minor_size, inner_table, twiddle, outer_table)


def finish_forward(part_real, part_imag, twiddle, outer_table):
    turn_cos = twiddle[0][:, :, None]
    turn_sin = twiddle[1][:, :, None]
    turned_real = part_real * turn_cos + part_imag * turn_sin
    turned_imag = part_imag * turn_cos - part_real * turn_sin
    outer_cos, outer_sin = outer_table
    spec_real = jnp.einsum("anc,nk->akc", turned_real, outer_cos, precision=HIGHEST) + jnp.einsum(
        "anc,nk->akc", turned_imag, outer_sin, precision=HIGHEST
    )
    spec_imag = jnp.einsum("anc,nk->akc", turned_imag, outer_cos, precision=HIGHEST) - jnp.einsum(
        "anc,nk->akc", turned_real, outer_sin, precision=HIGHEST
    )
    return (spec_real, spec_imag)


def forward_signal(signal, tables):
    major_size, minor_size, inner_table, twiddle, outer_table = tables
    channels = signal.shape[1]
    flattened = signal.reshape(major_size // 2, minor_size * channels)
    inner_cos = inner_table[0][:, : major_size // 2]
    inner_sin = inner_table[1][:, : major_size // 2]
    part_real = jnp.dot(inner_cos, flattened, precision=HIGHEST).reshape(
        major_size, minor_size, channels
    )
    part_imag = -jnp.dot(inner_sin, flattened, precision=HIGHEST).reshape(
        major_size, minor_size, channels
    )
    return finish_forward(part_real, part_imag, twiddle, outer_table)


def forward_taps(circular_taps, tables):
    major_size, minor_size, inner_table, twiddle, outer_table = tables
    channels = circular_taps.shape[1]
    flattened = circular_taps.reshape(major_size, minor_size * channels)
    part_real = jnp.dot(inner_table[0], flattened, precision=HIGHEST).reshape(
        major_size, minor_size, channels
    )
    part_imag = -jnp.dot(inner_table[1], flattened, precision=HIGHEST).reshape(
        major_size, minor_size, channels
    )
    return finish_forward(part_real, part_imag, twiddle, outer_table)


def inverse(spec_real, spec_imag, tables):
    major_size, minor_size, inner_table, twiddle, outer_table = tables
    channels = spec_real.shape[2]
    outer_cos, outer_sin = outer_table
    back_real = jnp.einsum("akc,kn->anc", spec_real, outer_cos, precision=HIGHEST) - jnp.einsum(
        "akc,kn->anc", spec_imag, outer_sin, precision=HIGHEST
    )
    back_imag = jnp.einsum("akc,kn->anc", spec_imag, outer_cos, precision=HIGHEST) + jnp.einsum(
        "akc,kn->anc", spec_real, outer_sin, precision=HIGHEST
    )
    turn_cos = twiddle[0][:, :, None]
    turn_sin = twiddle[1][:, :, None]
    turned_real = (back_real * turn_cos - back_imag * turn_sin).reshape(
        major_size, minor_size * channels
    )
    turned_imag = (back_imag * turn_cos + back_real * turn_sin).reshape(
        major_size, minor_size * channels
    )
    half_rows = major_size // 2
    values = jnp.dot(inner_table[0][:half_rows], turned_real, precision=HIGHEST) - jnp.dot(
        inner_table[1][:half_rows], turned_imag, precision=HIGHEST
    )
    return values.reshape(half_rows * minor_size, channels) / (major_size * minor_size)


def two_sided(signal, forward, backward, skip_gain, tables):
    circular_taps = jnp.concatenate([forward, jnp.zeros_like(forward[:1]), backward[:0:-1]], axis=0)
    signal_real, signal_imag = forward_signal(signal, tables)
    taps_real, taps_imag = forward_taps(circular_taps, tables)
    prod_real = signal_real * taps_real - signal_imag * taps_imag
    prod_imag = signal_real * taps_imag + signal_imag * taps_real
    return inverse(prod_real, prod_imag, tables) + signal * skip_gain


def channel_taps(hidden, position_ramp, filter_weight, deltas):
    window = jnp.exp(-position_ramp * deltas[None, :])
    pairs = []
    for order_index in range(filter_weight.shape[0]):
        forward = jnp.dot(hidden, filter_weight[order_index, 0], precision=HIGHEST) * window
        backward = jnp.dot(hidden, filter_weight[order_index, 1], precision=HIGHEST) * window
        pairs.append((forward, backward))
    return pairs


def general_local(
    tokens,
    norm_gain,
    first_gate,
    second_gate,
    value_weight,
    short_weight,
    short_bias,
    embed_weight,
    embed_bias,
    inner_weight,
    inner_bias,
    filter_freq,
    filter_weight,
    filter_skip,
    output_gain,
    output_weight,
):
    row_count = lax.axis_size("row")
    row_index = lax.axis_index("row")
    col_index = lax.axis_index("col")
    local_tokens = tokens.shape[0]
    length = local_tokens * row_count
    col_width = first_gate.shape[1]
    own_width = col_width // row_count
    widened = tokens.astype(jnp.float32)
    normed = (
        widened
        * lax.rsqrt(jnp.mean(widened * widened, axis=1, keepdims=True) + NORM_EPS)
        * norm_gain
    ).astype(jnp.bfloat16)
    gate_first = jnp.dot(normed, first_gate, preferred_element_type=jnp.float32).astype(
        jnp.bfloat16
    )
    gate_second = jnp.dot(normed, second_gate, preferred_element_type=jnp.float32).astype(
        jnp.bfloat16
    )
    gate_value = jnp.dot(normed, value_weight, preferred_element_type=jnp.float32).astype(
        jnp.bfloat16
    )
    position_ramp, hidden = filter_hidden(
        length, embed_weight, embed_bias, inner_weight, inner_bias, filter_freq
    )
    channel_start = (col_index * row_count + row_index) * own_width
    deltas = lax.dynamic_slice_in_dim(decay_rates(), channel_start, own_width)
    tap_pairs = channel_taps(hidden, position_ramp, filter_weight, deltas)
    tables = make_tables(2 * length)
    half_width = short_weight.shape[1] // 2
    moved = (
        lax.all_to_all(gate_first, "row", split_axis=1, concat_axis=0, tiled=True),
        lax.all_to_all(gate_second, "row", split_axis=1, concat_axis=0, tiled=True),
        lax.all_to_all(gate_value, "row", split_axis=1, concat_axis=0, tiled=True),
    )
    weights_own = lax.dynamic_slice_in_dim(short_weight, row_index * own_width, own_width, 2)
    bias_own = lax.dynamic_slice_in_dim(short_bias, row_index * own_width, own_width, 1)
    smoothed = [
        short_filter(
            jnp.pad(moved[branch], ((half_width, half_width), (0, 0))),
            weights_own[branch],
            bias_own[branch],
            length,
        )
        for branch in range(3)
    ]
    signal = smoothed[2]
    for order_index in range(2):
        signal = smoothed[order_index] * two_sided(
            signal,
            tap_pairs[order_index][0],
            tap_pairs[order_index][1],
            filter_skip[order_index],
            tables,
        )
    result = jax.tree.map(
        lambda part, own: part.astype(own.dtype),
        lax.all_to_all(for_sending(signal), "row", split_axis=0, concat_axis=1, tiled=True),
        signal,
    )
    group_width = CHANNELS // GROUPS
    grouped = result.reshape(local_tokens, col_width // group_width, group_width)
    scaled = grouped * lax.rsqrt(jnp.mean(grouped * grouped, axis=2, keepdims=True) + NORM_EPS)
    mix_local = (scaled.reshape(local_tokens, col_width) * output_gain).astype(jnp.bfloat16)
    gathered = lax.all_to_all(mix_local, "col", split_axis=0, concat_axis=1, tiled=True)
    return jnp.dot(gathered, output_weight, preferred_element_type=jnp.float32).astype(jnp.bfloat16)


LANES = 128
SUBLANES = 16
BF16 = jnp.bfloat16
F32 = jnp.float32


def fast_tables(length, rows, tile_rows, own):
    total = 2 * length
    majors = length // LANES
    n1 = (np.arange(rows)[None, :] * tile_rows + np.arange(tile_rows)[:, None]).reshape(-1)
    k1 = np.arange(majors) + 0.5
    angle = 2.0 * np.pi * np.outer(k1, n1) / (2 * majors)
    eye = np.eye(own)
    inner = np.concatenate([np.kron(np.cos(angle), eye), np.kron(-np.sin(angle), eye)], 0)
    inner_back = inner.T * (2.0 / total)
    n2 = np.arange(LANES)
    turn = np.repeat(2.0 * np.pi * np.outer(k1, n2) / total, own, axis=0)
    twiddle = np.stack([np.cos(turn), np.sin(turn)])
    phase = 2.0 * np.pi * (np.outer(n2, n2) % LANES) / LANES
    c, s = np.cos(phase), np.sin(phase)
    outer = np.block([[c, -s], [s, c]])
    ramp = np.linspace(0.0, 1.0, length)
    angles = 2.0 * np.pi * np.arange(length) / length
    bands = np.linspace(0.0001, FREQ_BANDS - 1, FREQ_BANDS)[:, None]
    feats = np.concatenate([ramp[None], np.cos(bands * angles), -np.sin(bands * angles)], 0)
    feats = np.pad(feats, ((0, -feats.shape[0] % SUBLANES), (0, 0))).astype(np.float32)
    high = feats.astype(BF16)
    low = (feats - high.astype(np.float32)).astype(BF16)
    return (
        jnp.asarray(inner, BF16),
        jnp.asarray(inner_back, BF16),
        jnp.asarray(twiddle, F32),
        jnp.asarray(outer, BF16),
        jnp.asarray(outer.T, BF16),
        jnp.asarray(np.concatenate([high, low, high], 0)),
    )


def bounded_sin(x):
    turns = jnp.round(x * (1.0 / math.pi))
    r = x - turns * 3.140625
    r = r - turns * 9.67502593994140625e-4
    r = r - turns * 1.509957990978376432e-7
    half = turns * 0.5
    sign = 1.0 - 4.0 * (half - jnp.floor(half))
    q = r * r
    p = -2.5052108385e-8 + q * 1.6059043837e-10
    p = 2.7557319224e-6 + q * p
    p = -1.9841269841e-4 + q * p
    p = 8.3333333333e-3 + q * p
    p = -1.6666666667e-1 + q * p
    return sign * (r + r * q * p)


def mm(a, b):
    return jnp.dot(a.astype(BF16), b.astype(BF16), preferred_element_type=F32)


def halves(x):
    high = x.astype(BF16).astype(F32)
    return high, x - high


def tdot(a, stacked):
    high, low = halves(a)
    return lax.dot_general(
        jnp.concatenate([high, high, low], 0).astype(BF16),
        stacked,
        (((0,), (0,)), ((), ())),
        preferred_element_type=F32,
    )


def stack(b):
    high, low = halves(b)
    return jnp.concatenate([high, low, high], 0).astype(BF16)


def column(row, start, count):
    shape = (count, row.shape[1])
    hit = lax.broadcasted_iota(jnp.int32, shape, 1) == start + lax.broadcasted_iota(
        jnp.int32, shape, 0
    )
    return jnp.sum(jnp.where(hit, row.astype(F32), 0.0), axis=1, keepdims=True)


SMALL = 11


def fast_kernel(dims, *refs):
    tokens_h, first_h, second_h, value_h, out_w_h = refs[:5]
    small_h = refs[5 : 5 + SMALL]
    inner_h, inner_back_h, twiddle_h, outer_h, outer_back_h, feats_h, out_ref = refs[
        5 + SMALL : 12 + SMALL
    ]
    tokens_v, gates_v, out_w_v = refs[12 + SMALL : 15 + SMALL]
    small_v = refs[15 + SMALL : 15 + 2 * SMALL]
    (
        norm_gain, short_weight, short_bias, embed_weight, embed_bias, inner_weight,
        inner_bias, filter_freq, filter_weight, filter_skip, output_gain,
    ) = small_v
    (
        inner_v, inner_back_v, twiddle_v, outer_v, outer_back_v, feats_v, normed_v,
        send_a, recv_a, send_b, recv_b, send_s, recv_s, second_v, send_h, recv_h, gains,
        gain_map, spectra, embed_pad, load_sem, small_sem, send_a_sem, recv_a_sem, send_b_sem,
        recv_b_sem, send_g_sem, recv_g_sem, send_s_sem, recv_s_sem, send_h_sem, recv_h_sem,
    ) = refs[15 + 2 * SMALL :]
    rows_n, cols_n, block, own = dims
    length = rows_n * block
    tiles = block // LANES
    piece = block // cols_n
    groups = LANES // piece
    half = own // groups
    row_me = lax.axis_index("row")
    col_me = lax.axis_index("col")
    me = row_me * cols_n + col_me
    everyone = rows_n * cols_n

    loads = [
        (tokens_h, tokens_v),
        (value_h, gates_v.at[2]),
        (first_h, gates_v.at[0]),
        (second_h, gates_v.at[1]),
        (feats_h, feats_v),
        (inner_h, inner_v),
        (twiddle_h, twiddle_v),
        (outer_h, outer_v),
        (outer_back_h, outer_back_v),
        (inner_back_h, inner_back_v),
    ] + [(out_w_h.at[:, g], out_w_v.at[g]) for g in range(groups)]
    copies = [
        pltpu.make_async_copy(src, dst, load_sem.at[i]) for i, (src, dst) in enumerate(loads)
    ]
    smalls = [
        pltpu.make_async_copy(src, dst, small_sem.at[i])
        for i, (src, dst) in enumerate(zip(small_h, small_v))
    ]
    copies[0].start()
    smalls[0].start()
    copies[1].start()

    def place(flat):
        return (lax.div(flat, cols_n), lax.rem(flat, cols_n))

    barrier = pltpu.get_barrier_semaphore()
    for step in range(1, everyone):
        pl.semaphore_signal(
            barrier,
            inc=1,
            device_id=place(lax.rem(me + step, everyone)),
            device_id_type=pl.DeviceIdType.MESH,
        )

    for copy in copies[2:10] + smalls[1:]:
        copy.start()
    copies[0].wait()
    smalls[0].wait()
    gain_row = norm_gain[...]
    chunk = 32
    for start in range(0, block, chunk):
        x = tokens_v[start : start + chunk, :].astype(F32)
        scale = lax.rsqrt(jnp.mean(x * x, axis=1, keepdims=True) + NORM_EPS)
        normed_v[start : start + chunk, :] = (x * scale * gain_row).astype(BF16)

    MESH = pl.DeviceIdType.MESH
    sends = []

    def project(order, branch):
        copies[1 + order].wait()
        gate = jnp.dot(normed_v[...], gates_v[branch], preferred_element_type=F32)
        send_a[order] = gate.T.astype(BF16).reshape(rows_n, own, block)
        if order == 0:
            pl.semaphore_wait(barrier, everyone - 1)
        for step in range(1, rows_n):
            peer = lax.rem(row_me + step, rows_n)
            copy = pltpu.make_async_remote_copy(
                src_ref=send_a.at[order, peer],
                dst_ref=recv_a.at[order, row_me],
                send_sem=send_a_sem.at[order, step],
                recv_sem=recv_a_sem.at[order, step],
                device_id=(peer, col_me),
                device_id_type=MESH,
            )
            copy.start()
            sends.append((order, copy))
        recv_a[order, row_me] = send_a[order, row_me]

    project(0, 2)
    project(1, 0)
    copies[3].wait()
    gate = jnp.dot(normed_v[...], gates_v[1], preferred_element_type=F32)
    gate = gate.astype(BF16).astype(F32)
    second_v[...] = gate.T
    send_h[0] = gate[:1]
    send_h[1] = gate[block - 1 :]
    halo_sends = []
    for edge, shift in ((0, rows_n - 1), (1, 1)):
        copy = pltpu.make_async_remote_copy(
            src_ref=send_h.at[edge],
            dst_ref=recv_h.at[edge],
            send_sem=send_h_sem.at[edge],
            recv_sem=recv_h_sem.at[edge],
            device_id=(lax.rem(row_me + shift, rows_n), col_me),
            device_id_type=MESH,
        )
        copy.start()
        halo_sends.append(copy)
    for copy in copies[10:]:
        copy.start()
    for copy in smalls[1:]:
        copy.wait()

    gain_sends = []
    gains[col_me] = output_gain[...]
    for step in range(1, cols_n):
        copy = pltpu.make_async_remote_copy(
            src_ref=output_gain,
            dst_ref=gains.at[col_me],
            send_sem=send_g_sem.at[step],
            recv_sem=recv_g_sem.at[step],
            device_id=(row_me, lax.rem(col_me + step, cols_n)),
            device_id_type=pl.DeviceIdType.MESH,
        )
        copy.start()
        gain_sends.append(copy)

    def to_layout(x):
        return jnp.concatenate(
            [
                jnp.concatenate(
                    [
                        x[:, g * half : (g + 1) * half, j * LANES : (j + 1) * LANES].reshape(
                            rows_n * half, LANES
                        )
                        for g in range(groups)
                    ],
                    axis=1,
                )
                for j in range(tiles)
            ],
            axis=0,
        )

    def taps_layout(x):
        return jnp.concatenate(
            [
                jnp.concatenate(
                    [
                        x[
                            g * half : (g + 1) * half,
                            (r * tiles + j) * LANES : (r * tiles + j + 1) * LANES,
                        ]
                        for g in range(groups)
                    ],
                    axis=1,
                )
                for j in range(tiles)
                for r in range(rows_n)
            ],
            axis=0,
        )

    freq = column(filter_freq[...], 0, filter_freq.shape[1])
    copies[4].wait()
    embed_pad[...] = jnp.zeros_like(embed_pad)
    embed_pad[: embed_weight.shape[0], :] = embed_weight[...]
    hidden = bounded_sin(
        freq
        * (
            tdot(embed_pad[...], feats_v[...])
            + column(embed_bias[...], 0, embed_bias.shape[1])
        )
    )
    hidden = bounded_sin(
        freq * (tdot(inner_weight[...], stack(hidden)) + column(inner_bias[...], 0, inner_bias.shape[1]))
    )
    channels = rows_n * cols_n * own
    slowest = math.log(DECAY_TARGET) / SLOW_SPAN
    fastest = math.log(DECAY_TARGET) / FAST_SPAN
    channel = (
        (col_me * rows_n + row_me) * own + lax.broadcasted_iota(jnp.int32, (own, 1), 0)
    ).astype(F32)
    decay = jnp.abs(slowest + channel * ((fastest - slowest) / (channels - 1)))
    lag = lax.broadcasted_iota(jnp.int32, (own, length), 1)
    window = jnp.exp(-(lag.astype(F32) * (1.0 / (length - 1))) * decay)
    for copy in copies[5:8]:
        copy.wait()

    def twist(real, imag, sign):
        cos = jnp.concatenate([twiddle_v[0]] * groups, axis=1)
        sin = jnp.concatenate([twiddle_v[1]] * groups, axis=1) * sign
        return real * cos + imag * sin, imag * cos - real * sin

    def lanes_of(x, g):
        return x[:, g * LANES : (g + 1) * LANES]

    def forward_inner(x):
        part = mm(inner_v[...], x)
        count = part.shape[0] // 2
        return twist(part[:count], part[count:], 1.0)

    high, low = halves(filter_weight[...].reshape(4 * own, filter_weight.shape[3]))
    taps = jnp.dot(
        jnp.concatenate([high, high, low], 1).astype(BF16),
        stack(hidden),
        preferred_element_type=F32,
    )
    for order in range(2):
        fwd = taps[2 * order * own : (2 * order + 1) * own] * window
        bwd = taps[(2 * order + 1) * own : (2 * order + 2) * own] * window
        bwd = jnp.where(lag == 0, 0.0, bwd)
        plus = forward_inner(taps_layout(fwd + bwd))
        minus = forward_inner(taps_layout(fwd - bwd))
        for g in range(groups):
            p = jnp.concatenate([lanes_of(plus[0], g), lanes_of(plus[1], g)], axis=1)
            m = jnp.concatenate([lanes_of(minus[0], g), lanes_of(minus[1], g)], axis=1)
            spectra[order, g, :, :LANES] = mm(p, outer_v[:, :LANES])
            spectra[order, g, :, LANES:] = mm(m, outer_v[:, LANES:])

    width = rows_n * own
    count = rows_n * half
    second_sends = []

    def send_second():
        for copy in halo_sends:
            copy.wait_recv()
        x = second_v[...]
        spot = lax.broadcasted_iota(jnp.int32, (width, block), 1)
        first_col = jnp.where(row_me == 0, 0.0, column(recv_h[1], 0, width))
        last_col = jnp.where(row_me == rows_n - 1, 0.0, column(recv_h[0], 0, width))
        before = jnp.where(spot == 0, first_col, pltpu.roll(x, 1, 1))
        after = jnp.where(spot == block - 1, last_col, pltpu.roll(x, block - 1, 1))
        w = [column(short_weight[1, j : j + 1, :], 0, width) for j in range(3)]
        x = column(short_bias[1:2, :], 0, width) + before * w[0] + x * w[1] + after * w[2]
        x = x.reshape(rows_n, groups, half, block)
        for q in range(cols_n):
            part = jnp.concatenate(
                [x[:, g, :, q * piece : (q + 1) * piece].reshape(count, piece) for g in range(groups)],
                axis=1,
            )
            send_s[q] = part.astype(BF16)
        recv_s[col_me] = send_s[col_me]
        for step in range(1, cols_n):
            peer = lax.rem(col_me + step, cols_n)
            copy = pltpu.make_async_remote_copy(
                src_ref=send_s.at[peer],
                dst_ref=recv_s.at[col_me],
                send_sem=send_s_sem.at[step],
                recv_sem=recv_s_sem.at[step],
                device_id=(row_me, peer),
                device_id_type=MESH,
            )
            copy.start()
            second_sends.append(copy)

    for copy in copies[8:10]:
        copy.wait()
    pos = lax.broadcasted_iota(jnp.int32, (rows_n, own, block), 2)

    def smooth(slot, branch):
        for b, copy in sends:
            if b == slot:
                copy.wait_recv()
        x = recv_a[slot].astype(F32)
        flat = x.reshape(rows_n * own, block)
        before = pltpu.roll(flat, 1, 1).reshape(rows_n, own, block)
        after = pltpu.roll(flat, block - 1, 1).reshape(rows_n, own, block)
        gap = jnp.zeros((1, own, block), F32)
        before = jnp.where(pos == 0, jnp.concatenate([gap, before[:-1]], 0), before)
        after = jnp.where(pos == block - 1, jnp.concatenate([after[1:], gap], 0), after)
        start = row_me * own
        w = [
            column(short_weight[branch, j : j + 1, :], start, own).reshape(1, own, 1)
            for j in range(3)
        ]
        bias = column(short_bias[branch : branch + 1, :], start, own).reshape(1, own, 1)
        return to_layout(bias + before * w[0] + x * w[1] + after * w[2])

    signal = smooth(0, 2)
    for order in range(2):
        real, imag = forward_inner(signal)
        back_real, back_imag = [], []
        for g in range(groups):
            t = jnp.concatenate([lanes_of(real, g), lanes_of(imag, g)], axis=1)
            spec = mm(t, outer_v[...])
            sr, si = spec[:, :LANES], spec[:, LANES:]
            hr, hi = spectra[order, g, :, :LANES], spectra[order, g, :, LANES:]
            prod = jnp.concatenate([sr * hr - si * hi, sr * hi + si * hr], axis=1)
            back = mm(prod, outer_back_v[...])
            back_real.append(back[:, :LANES])
            back_imag.append(back[:, LANES:])
        ur, ui = twist(jnp.concatenate(back_real, 1), jnp.concatenate(back_imag, 1), -1.0)
        conv = mm(inner_back_v[...], jnp.concatenate([ur, ui], axis=0))
        skip = column(filter_skip[order : order + 1, :], 0, own)
        skip = to_layout(jnp.broadcast_to(skip[None], (rows_n, own, block)))
        signal = conv + signal * skip
        if order == 0:
            signal = signal * smooth(1, 0)

    for j in range(tiles):
        for h in range(LANES // piece):
            part = jnp.concatenate(
                [
                    signal[
                        j * count : (j + 1) * count,
                        g * LANES + h * piece : g * LANES + (h + 1) * piece,
                    ]
                    for g in range(groups)
                ],
                axis=1,
            )
            send_b[j * (LANES // piece) + h] = part.astype(BF16).reshape(rows_n, half, LANES)
    last = []
    for step in range(1, everyone):
        row_to, col_to = place(lax.rem(me + step, everyone))
        copy = pltpu.make_async_remote_copy(
            src_ref=send_b.at[col_to, row_to],
            dst_ref=recv_b.at[col_me, row_me],
            send_sem=send_b_sem.at[step],
            recv_sem=recv_b_sem.at[step],
            device_id=(row_to, col_to),
            device_id_type=pl.DeviceIdType.MESH,
        )
        copy.start()
        last.append(copy)
    recv_b[col_me, row_me] = send_b[col_me, row_me]
    send_second()

    for copy in gain_sends:
        copy.wait_recv()
    lane = lax.broadcasted_iota(jnp.int32, (rows_n * half, LANES), 1)
    for q in range(cols_n):
        col_gain = column(gains[q], 0, width).reshape(rows_n, own, 1)
        result = jnp.zeros((rows_n * half, LANES), F32)
        for g in range(groups):
            part = col_gain[:, g * half : (g + 1) * half].reshape(rows_n * half, 1)
            result = jnp.where(lax.div(lane, piece) == g, part, result)
        gain_map[q] = result
    for copy in copies[10:]:
        copy.wait()
    for copy in second_sends + last:
        copy.wait_recv()

    group_width = CHANNELS // GROUPS
    per_group = group_width // own
    turned = []
    for q in range(cols_n):
        for r in range(0, rows_n, per_group):
            x = recv_b[q, r : r + per_group].astype(F32).reshape(per_group * half, LANES)
            x = x * recv_s[q, r * half : (r + per_group) * half, :].astype(F32)
            total = jnp.sum(x * x, axis=0, keepdims=True)
            square = total
            for g in range(1, groups):
                square = square + pltpu.roll(total, g * piece, 1)
            scale = lax.rsqrt(square * (1.0 / group_width) + NORM_EPS)
            gain = gain_map[q, r * half : (r + per_group) * half, :]
            turned.append(x * scale * gain)
    mixed = jnp.concatenate(turned, axis=0).T.astype(BF16)
    depth = everyone * half
    step_width = 512
    for start in range(0, out_ref.shape[1], step_width):
        acc = jnp.zeros((piece, step_width), F32)
        for g in range(groups):
            acc = acc + jnp.dot(
                mixed[g * piece : (g + 1) * piece],
                out_w_v[g, :, :, start : start + step_width].reshape(depth, step_width),
                preferred_element_type=F32,
            )
        out_ref[:, start : start + step_width] = acc.astype(BF16)

    for _, copy in sends:
        copy.wait_send()
    for copy in halo_sends + gain_sends + second_sends + last:
        copy.wait_send()


def fast_local(*args):
    (
        tokens, norm_gain, first_gate, second_gate, value_weight, short_weight, short_bias,
        embed_weight, embed_bias, inner_weight, inner_bias, filter_freq, filter_weight,
        filter_skip, output_gain, output_weight,
    ) = args
    rows_n, cols_n = lax.axis_size("row"), lax.axis_size("col")
    block, model = tokens.shape
    own = filter_weight.shape[3]
    piece = block // cols_n
    groups = LANES // piece
    half = own // groups
    tiles = block // LANES
    length = block * rows_n
    width = first_gate.shape[1]
    everyone = rows_n * cols_n
    tables = fast_tables(length, rows_n, tiles, half)
    out_width = output_weight.shape[1]
    out_w = output_weight.reshape(everyone, groups, half, out_width)
    vm = pl.BlockSpec(memory_space=pltpu.VMEM)
    hbm = pl.BlockSpec(memory_space=pl.ANY)
    small = [
        norm_gain.reshape(1, -1),
        short_weight,
        short_bias,
        embed_weight,
        embed_bias.reshape(1, -1),
        inner_weight,
        inner_bias.reshape(1, -1),
        filter_freq.reshape(1, -1),
        jnp.swapaxes(filter_weight, 2, 3),
        filter_skip,
        output_gain.reshape(1, -1),
    ]
    operands = [tokens, first_gate, second_gate, value_weight, out_w, *small, *tables]
    rows_all = tiles * rows_n * half
    DMA = pltpu.SemaphoreType.DMA
    return pl.pallas_call(
        functools.partial(fast_kernel, (rows_n, cols_n, block, own)),
        out_shape=pltpu.VMEM((piece, out_width), BF16),
        in_specs=[hbm] * len(operands),
        out_specs=vm,
        scratch_shapes=[
            pltpu.VMEM(tokens.shape, BF16),
            pltpu.VMEM((3, model, width), BF16),
            pltpu.VMEM((groups, everyone, half, out_width), BF16),
        ]
        + [pltpu.VMEM(array.shape, array.dtype) for array in small + list(tables)]
        + [
            pltpu.VMEM(tokens.shape, BF16),
            pltpu.VMEM((2, rows_n, own, block), BF16),
            pltpu.VMEM((2, rows_n, own, block), BF16),
            pltpu.VMEM((cols_n, rows_n, half, LANES), BF16),
            pltpu.VMEM((cols_n, rows_n, half, LANES), BF16),
            pltpu.VMEM((cols_n, rows_n * half, LANES), BF16),
            pltpu.VMEM((cols_n, rows_n * half, LANES), BF16),
            pltpu.VMEM((width, block), F32),
            pltpu.VMEM((2, 1, width), F32),
            pltpu.VMEM((2, 1, width), F32),
            pltpu.VMEM((cols_n, 1, width), F32),
            pltpu.VMEM((cols_n, rows_n * half, LANES), F32),
            pltpu.VMEM((2, groups, rows_all, 2 * LANES), F32),
            pltpu.VMEM((tables[-1].shape[0] // 3, embed_weight.shape[1]), F32),
            DMA((10 + groups,)),
            DMA((SMALL,)),
            DMA((2, rows_n)),
            DMA((2, rows_n)),
            DMA((everyone,)),
            DMA((everyone,)),
            DMA((cols_n,)),
            DMA((cols_n,)),
            DMA((cols_n,)),
            DMA((cols_n,)),
            DMA((2,)),
            DMA((2,)),
        ],
        compiler_params=pltpu.CompilerParams(
            collective_id=0, has_side_effects=True, vmem_limit_bytes=56 * 1024 * 1024
        ),
    )(*operands)


def kernel_fits(tokens, filter_weight, rows_n, cols_n):
    block = tokens.shape[0]
    own = filter_weight.shape[3]
    piece = block // cols_n
    if block % LANES or LANES % piece:
        return False
    groups = LANES // piece
    return own % (groups * SUBLANES) == 0 and (CHANNELS // GROUPS) % own == 0


def local(*args):
    if kernel_fits(args[0], args[12], lax.axis_size("row"), lax.axis_size("col")):
        return fast_local(*args)
    return general_local(*args)


def solution(mesh):
    in_specs = (
        P("row", None),
        P(),
        P(None, "col"),
        P(None, "col"),
        P(None, "col"),
        P(None, None, "col"),
        P(None, "col"),
        P(),
        P(),
        P(),
        P(),
        P(),
        P(None, None, None, ("col", "row")),
        P(None, ("col", "row")),
        P("col"),
        P(),
    )
    out_specs = P(("row", "col"), None)
    return jax.shard_map(local, mesh=mesh, in_specs=in_specs, out_specs=out_specs, check_vma=False)
```

profile of v0, /device:TPU:1, one launch (start us, length us, event | category | flops | bytes accessed | tf_op | source)
XLA Modules:
  0.0 213.7 jit_solution(14069972327601891070)
XLA Ops:
  4.1 12.0 %all-to-all-start.2 = ((bf16[256,32,4]{0,2,1:T(4,128)(2,1)}), bf16[256,32,4]{0,2,1:T(4,128)(2,1)}, u32[]{:S(2)}, u32[]{:S(2)}) async-start(bf16[256,32,4]{0,2,1:T(4,128)(2,1)} %all_to_all.72), calls=%async_computation.2 | async-start | bytes 131072 | tf_op jit(solution)/shard_map/all_to_all | solution.py:227
  20.0 8.7 %fusion.3 = f32[8192,64]{0,1:T(8,128)S(1)} fusion(f32[33,64]{1,0:T(8,128)S(1)} %copy-done.8, f32[8192,16]{0,1:T(8,128)S(1)} %get-tuple-element.16, f32[8192,16]{0,1:T(8,128)S(1)} %get-tuple-element.15, f32[8192,1]{0,1:T(1,128)S(1)} %bitcast.258, f32[64]{0:T(128)S(1)} %copy-done.14, f32[64]{0:T(128)S(1)} %copy-done.11), kind=kOutput, calls=%fused_computation.5 | convolution fusion | flops 209207296 | bytes 3187456 | tf_op jit(solution)/shard_map/dot_general | solution.py:41
  28.7 8.9 %fusion.1 = f32[8192,64]{0,1:T(8,128)S(1)} fusion(f32[8192,64]{0,1:T(8,128)S(1)} %fusion.3, f32[64,64]{1,0:T(8,128)S(1)} %copy-done.7, f32[64]{0:T(128)S(1)} %copy-done.15, f32[64]{0:T(128)S(1)} %copy-done.11), kind=kOutput, calls=%fused_computation.2 | convolution fusion | flops 403701760 | bytes 4211200 | tf_op jit(solution)/shard_map/dot_general | solution.py:43
  40.1 12.5 %convolution_multiply_fusion.1 = f32[8192,4]{0,1:T(4,128)S(1)} fusion(f32[8192,64]{0,1:T(8,128)S(1)} %fusion.1, f32[4]{0:T(128)S(1)} %dynamic_slice.11, f32[8192]{0:T(1024)S(1)} %get-tuple-element.17, f32[2,2,64,4]{2,3,1,0:T(4,128)S(1)} %copy-done.9), kind=kOutput, calls=%fused_computation.7 | convolution fusion | flops 25231360 | bytes 2263552 | tf_op jit(solution)/shard_map/dot_general | solution.py:170
  54.1 5.6 %reverse = f32[8192,4]{0,1:T(4,128)S(1)} reverse(f32[8192,4]{0,1:T(4,128)S(1)} %bitcast.254), dimensions={0} | reverse | bytes 262144
  60.1 5.1 %copy.95 = f32[16384,4]{1,0:T(8,128)} copy(f32[16384,4]{0,1:T(4,128)S(1)} %concatenate.29) | data formatting | bytes 524288 | tf_op jit(solution)/shard_map/concatenate | solution.py:158
  65.2 8.3 %reshape.264 = f32[128,512]{1,0:T(8,128)S(1)} reshape(f32[16384,4]{1,0:T(8,128)} %copy.95) | data formatting | bytes 524288 | tf_op jit(solution)/shard_map/reshape | solution.py:122
  76.5 5.6 %reverse.1 = f32[8192,4]{0,1:T(4,128)S(1)} reverse(f32[8192,4]{0,1:T(4,128)S(1)} %bitcast.253), dimensions={0} | reverse | bytes 262144
  82.5 5.1 %copy.116 = f32[16384,4]{1,0:T(8,128)} copy(f32[16384,4]{0,1:T(4,128)S(1)} %concatenate.30) | data formatting | bytes 524288 | tf_op jit(solution)/shard_map/concatenate | solution.py:158
  87.6 8.3 %reshape.268 = f32[128,512]{1,0:T(8,128)S(1)} reshape(f32[16384,4]{1,0:T(8,128)} %copy.116) | data formatting | bytes 524288 | tf_op jit(solution)/shard_map/reshape | solution.py:122
  100.2 2.3 %convolution_convert_fusion.2 = bf16[256,128]{0,1:T(8,128)(2,1)} fusion(bf16[2048,128]{1,0:T(8,128)(2,1)} %param.18, bf16[256,2048]{1,0:T(8,128)(2,1)S(1)} %copy-done.1, f32[2048]{0:T(1024)S(1)} %copy-done.18, f32[256]{0:T(256)S(1)} %add_rsqrt_fusion.1), kind=kOutput, calls=%fused_computation.44 | convolution fusion | flops 136347648 | bytes 1647616 | tf_op jit(solution)/shard_map/dot_general | solution.py:207
  108.3 9.6 %all-to-all-start.1 = ((bf16[256,32,4]{0,2,1:T(4,128)(2,1)}), bf16[256,32,4]{0,2,1:T(4,128)(2,1)S(1)}, u32[]{:S(2)}, u32[]{:S(2)}) async-start(bf16[256,32,4]{0,2,1:T(4,128)(2,1)} %all_to_all.68), calls=%async_computation.1 | async-start | bytes 131072 | tf_op jit(solution)/shard_map/all_to_all | solution.py:225
  119.0 2.6 %copy.89 = f32[8192,4]{1,0:T(8,128)} copy(f32[8192,4]{0,1:T(4,128)S(1)} %multiply_add_fusion.8) | data formatting | bytes 262144 | tf_op jit(solution)/shard_map/add | solution.py:56
  121.6 5.0 %reshape.263 = f32[64,512]{1,0:T(8,128)S(1)} reshape(f32[8192,4]{1,0:T(8,128)} %copy.89) | data formatting | bytes 262144 | tf_op jit(solution)/shard_map/reshape | solution.py:107
  134.7 5.7 %div.58 = f32[8192,4]{1,0:T(8,128)} reshape(f32[64,512]{1,0:T(8,128)S(1)} %fusion.17) | data formatting | bytes 262144 | tf_op jit(solution)/shard_map/div | solution.py:154
  140.3 2.8 %copy.111 = f32[8192,4]{0,1:T(4,128)S(1)} copy(f32[8192,4]{1,0:T(8,128)} %div.58) | data formatting | bytes 262144 | tf_op jit(solution)/shard_map/div | solution.py:154
  143.2 9.5 %all-to-all-start = ((bf16[256,32,4]{0,2,1:T(4,128)(2,1)}), bf16[256,32,4]{0,2,1:T(4,128)(2,1)S(1)}, u32[]{:S(2)}, u32[]{:S(2)}) async-start(bf16[256,32,4]{0,2,1:T(4,128)(2,1)} %all_to_all.64), calls=%async_computation | async-start | bytes 131072 | tf_op jit(solution)/shard_map/all_to_all | solution.py:226
  154.0 2.6 %copy.112 = f32[8192,4]{1,0:T(8,128)} copy(f32[8192,4]{0,1:T(4,128)S(1)} %add_multiply_fusion) | data formatting | bytes 262144 | tf_op jit(solution)/shard_map/mul | solution.py:242
  156.6 4.9 %reshape.267 = f32[64,512]{1,0:T(8,128)S(1)} reshape(f32[8192,4]{1,0:T(8,128)} %copy.112) | data formatting | bytes 262144 | tf_op jit(solution)/shard_map/reshape | solution.py:107
  169.6 5.7 %div.60 = f32[8192,4]{1,0:T(8,128)} reshape(f32[64,512]{1,0:T(8,128)S(1)} %fusion.16) | data formatting | bytes 262144 | tf_op jit(solution)/shard_map/div | solution.py:154
  175.3 2.9 %copy.132 = f32[8192,4]{0,1:T(4,128)S(1)} copy(f32[8192,4]{1,0:T(8,128)} %div.60) | data formatting | bytes 262144 | tf_op jit(solution)/shard_map/div | solution.py:154
  178.3 17.8 %all_to_all.86 = bf16[32,256,4]{1,2,0:T(4,128)(2,1)S(1)} all-to-all(bf16[32,256,4]{1,2,0:T(4,128)(2,1)S(1)} %bitcast.257), channel_id=1, replica_groups=mesh['row'=32,'col'=8] {'row'}, dimensions={0} | all-to-all | bytes 131072 | tf_op jit(solution)/shard_map/all_to_all | solution.py:251
  196.9 12.9 %all_to_all.87 = bf16[8,32,128]{2,1,0:T(8,128)(2,1)S(1)} all-to-all(bf16[8,32,128]{2,1,0:T(8,128)(2,1)S(1)} %copy.134), channel_id=1, replica_groups=mesh['row'=32,'col'=8] {'col'}, dimensions={0} | all-to-all | bytes 131072 | tf_op jit(solution)/shard_map/all_to_all | solution.py:258
  209.8 3.7 %convolution_convert_fusion = bf16[32,2048]{1,0:T(8,128)(2,1)} fusion(bf16[1024,2048]{1,0:T(8,128)(2,1)} %param.31, bf16[8,32,128]{2,1,0:T(8,128)(2,1)S(1)} %all_to_all.87), kind=kOutput, calls=%fused_computation.10 | convolution fusion | flops 134283264 | bytes 4390912 | tf_op jit(solution)/shard_map/dot_general | solution.py:259
  (132 shorter events, 44.6 us)
Async XLA Ops:
  0.0 1.6 copy-start
  1.6 18.4 %copy-start.8 = (f32[33,64]{1,0:T(8,128)S(1)}, f32[33,64]{1,0:T(8,128)}, u32[]{:S(2)}) copy-start(f32[33,64]{1,0:T(8,128)} %param.23) | copy-start | bytes 25348
  1.6 18.4 %copy-start.11 = (f32[64]{0:T(128)S(1)}, f32[64]{0:T(128)}, u32[]{:S(2)}) copy-start(f32[64]{0:T(128)} %param.27) | copy-start | bytes 772
  1.6 18.4 %copy-start.14 = (f32[64]{0:T(128)S(1)}, f32[64]{0:T(128)}, u32[]{:S(2)}) copy-start(f32[64]{0:T(128)} %param.24) | copy-start | bytes 772
  4.1 104.2 %all-to-all-start.2 = ((bf16[256,32,4]{0,2,1:T(4,128)(2,1)}), bf16[256,32,4]{0,2,1:T(4,128)(2,1)}, u32[]{:S(2)}, u32[]{:S(2)}) async-start(bf16[256,32,4]{0,2,1:T(4,128)(2,1)} %all_to_all.72), calls=%async_computation.2 | async-start | bytes 131072 | tf_op jit(solution)/shard_map/all_to_all | solution.py:227
  18.0 10.7 %copy-start.7 = (f32[64,64]{1,0:T(8,128)S(1)}, f32[64,64]{1,0:T(8,128)}, u32[]{:S(2)}) copy-start(f32[64,64]{1,0:T(8,128)} %param.25) | copy-start | bytes 49156
  18.0 10.7 %copy-start.15 = (f32[64]{0:T(128)S(1)}, f32[64]{0:T(128)}, u32[]{:S(2)}) copy-start(f32[64]{0:T(128)} %param.26) | copy-start | bytes 772
  28.7 9.0 %copy-start.9 = (f32[2,2,64,4]{2,3,1,0:T(4,128)S(1)}, f32[2,2,64,4]{2,3,1,0:T(4,128)}, u32[]{:S(2)}) copy-start(f32[2,2,64,4]{2,3,1,0:T(4,128)} %param.28) | copy-start | bytes 12292
  96.0 4.2 %copy-start.1 = (bf16[256,2048]{1,0:T(8,128)(2,1)S(1)}, bf16[256,2048]{1,0:T(8,128)(2,1)}, u32[]{:S(2)}) copy-start(bf16[256,2048]{1,0:T(8,128)(2,1)} %param.16) | copy-start | bytes 3145732
  96.0 4.2 %copy-start.18 = (f32[2048]{0:T(1024)S(1)}, f32[2048]{0:T(1024)}, u32[]{:S(2)}) copy-start(f32[2048]{0:T(1024)} %param.17) | copy-start | bytes 24580
  100.2 2.3 %copy-start.17 = (bf16[2048,128]{1,0:T(8,128)(2,1)S(1)}, bf16[2048,128]{1,0:T(8,128)(2,1)}, u32[]{:S(2)}) copy-start(bf16[2048,128]{1,0:T(8,128)(2,1)} %param.19) | copy-start | bytes 1572868
  102.5 2.6 %copy-start.3 = (f32[128,128,4]{1,0,2:T(8,128)S(1)}, f32[128,128,4]{1,0,2:T(8,128)}, u32[]{:S(2)}) copy-start(f32[128,128,4]{1,0,2:T(8,128)} %fusion.62) | copy-start | bytes 786436
  103.7 2.1 copy-start.2
  103.7 2.8 %copy-start.12 = (f32[3,128]{1,0:T(4,128)S(1)}, f32[3,128]{1,0:T(4,128)}, u32[]{:S(2)}) copy-start(f32[3,128]{1,0:T(4,128)} %param.22) | copy-start | bytes 4612
  103.7 2.9 %copy-start.13 = (f32[2,4]{1,0:T(2,128)S(1)}, f32[2,4]{1,0:T(2,128)}, u32[]{:S(2)}) copy-start(f32[2,4]{1,0:T(2,128)} %param.29) | copy-start | bytes 100
  103.7 2.9 %copy-start.10 = (bf16[3,3,128]{2,1,0:T(4,128)(2,1)S(1)}, bf16[3,3,128]{2,1,0:T(4,128)(2,1)}, u32[]{:S(2)}) copy-start(bf16[3,3,128]{2,1,0:T(4,128)(2,1)} %param.21) | copy-start | bytes 6916
  104.4 2.3 %copy-start.6 = (bf16[256,128]{0,1:T(8,128)(2,1)S(1)}, bf16[256,128]{0,1:T(8,128)(2,1)}, u32[]{:S(2)}) copy-start(bf16[256,128]{0,1:T(8,128)(2,1)} %convolution_convert_fusion.2) | copy-start | bytes 196612
  104.4 2.9 %copy-start.5 = (bf16[256,128]{0,1:T(8,128)(2,1)S(1)}, bf16[256,128]{0,1:T(8,128)(2,1)}, u32[]{:S(2)}) copy-start(bf16[256,128]{0,1:T(8,128)(2,1)} %convolution_convert_fusion.3) | copy-start | bytes 196612
  108.3 34.9 %all-to-all-start.1 = ((bf16[256,32,4]{0,2,1:T(4,128)(2,1)}), bf16[256,32,4]{0,2,1:T(4,128)(2,1)S(1)}, u32[]{:S(2)}, u32[]{:S(2)}) async-start(bf16[256,32,4]{0,2,1:T(4,128)(2,1)} %all_to_all.68), calls=%async_computation.1 | async-start | bytes 131072 | tf_op jit(solution)/shard_map/all_to_all | solution.py:225
  121.6 5.7 %copy-start.4 = (f32[128,128]{0,1:T(8,128)S(1)}, f32[128,128]{0,1:T(8,128)}, u32[]{:S(2)}) copy-start(f32[128,128]{0,1:T(8,128)} %fusion.96) | copy-start | bytes 196612
  143.2 35.0 %all-to-all-start = ((bf16[256,32,4]{0,2,1:T(4,128)(2,1)}), bf16[256,32,4]{0,2,1:T(4,128)(2,1)S(1)}, u32[]{:S(2)}, u32[]{:S(2)}) async-start(bf16[256,32,4]{0,2,1:T(4,128)(2,1)} %all_to_all.64), calls=%async_computation | async-start | bytes 131072 | tf_op jit(solution)/shard_map/all_to_all | solution.py:226
  175.3 21.2 %copy-start.16 = (f32[128]{0:T(128)S(1)}, f32[128]{0:T(128)}, u32[]{:S(2)}) copy-start(f32[128]{0:T(128)} %param.30) | copy-start | bytes 1540
where the time goes:
time: 218 us; the launch traced here: 214 us
  local copies, waits for them, and re-layouts  75.2 us (34%)
  matrix products  67.1 us (31%)
  starting transfers between devices  31.1 us (14%)
  blocking collectives  30.7 us (14%)
  other arithmetic  8.72 us (4%)
    all_to_all x1, blocking collectives, general_local(): lax.all_to_all(for_sending(signal), 'row', split_axis=0, concat_axis=1, t...  17.8 us
    div x4, local copies, waits for them, and re-layouts, inverse(): values.reshape(half_rows * minor_size, channels) / (major_size * minor_size)  17 us
    reshape x2, local copies, waits for them, and re-layouts, forward_taps(): flattened = circular_taps.reshape(major_size, minor_size * channels)  16.7 us
    dot_general x2, matrix products, channel_taps(): jnp.dot(hidden, filter_weight[order_index, 0], precision=HIGHEST) * window  13.7 us
    all_to_all x1, blocking collectives, general_local(): lax.all_to_all(mix_local, 'col', split_axis=0, concat_axis=1, tiled=True)  12.9 us
    all_to_all x1, starting transfers between devices, general_local(): lax.all_to_all(gate_value, 'row', split_axis=1, concat_axis=0, tiled=True)  12 us
    unnamed x42, local copies, waits for them, and re-layouts  11.5 us
    concatenate x4, local copies, waits for them, and re-layouts, two_sided(): jnp.concatenate([forward, jnp.zeros_like(forward[:1]), backward[:0:-1]],...  10.7 us
  transfers between devices with their start and end apart: 3, of which 0 were waited for; matrix products, arithmetic and copies ran while one was open for 66% of the time, Pallas kernels for 0%

commit v1 on v0

v1 whole, which is shorter than its diff:
```python
import functools
import math

import jax
import jax.numpy as jnp
import numpy as np
from jax import lax
from jax.experimental import pallas as pl
from jax.experimental.pallas import tpu as pltpu
from jax.sharding import PartitionSpec as P

CHANNELS = 1024
FREQ_BANDS = 16
FEATURES = 33
NORM_EPS = 1e-06
DECAY_TARGET = 0.01
FAST_SPAN = 0.3
SLOW_SPAN = 1.5
LANES = 128
OWN = 4
FEATURE_ROWS = 48
BF16 = jnp.bfloat16
F32 = jnp.float32

SIN_COEFS = (
    6.283185280154403,
    -41.34168061334532,
    81.60247636883796,
    -76.5811726421402,
    39.75982706857711,
)


def fast_tables(length):
    total = 2 * length
    majors = length // LANES
    n1 = np.arange(majors)
    k1 = np.arange(majors) + 0.5
    angle = 2.0 * np.pi * np.outer(k1, n1) / (2 * majors)
    eye = np.eye(OWN)
    inner = np.concatenate([np.kron(np.cos(angle), eye), np.kron(-np.sin(angle), eye)], 0)
    inner_back = inner.T * (2.0 / total)
    n2 = np.arange(LANES)
    turn = np.repeat(2.0 * np.pi * np.outer(k1, n2) / total, OWN, axis=0)
    twiddle = np.stack([np.cos(turn), np.sin(turn)])
    phase = 2.0 * np.pi * (np.outer(n2, n2) % LANES) / LANES
    c, s = np.cos(phase), np.sin(phase)
    outer = np.block([[c, -s], [s, c]])
    ramp = np.linspace(0.0, 1.0, length)
    angles = 2.0 * np.pi * np.arange(length) / length
    bands = np.linspace(0.0001, FREQ_BANDS - 1, FREQ_BANDS)[:, None]
    feats = np.concatenate(
        [ramp[None], np.cos(bands * angles), -np.sin(bands * angles), np.ones((1, length))], 0
    )
    feats = np.pad(feats, ((0, FEATURE_ROWS - feats.shape[0]), (0, 0))).astype(np.float32)
    high = feats.astype(BF16)
    low = (feats - high.astype(np.float32)).astype(BF16)
    return (
        jnp.asarray(inner, BF16),
        jnp.asarray(inner_back, BF16),
        jnp.asarray(twiddle, F32),
        jnp.asarray(outer, BF16),
        jnp.asarray(outer.T, BF16),
        jnp.asarray(np.concatenate([high, low], 0)),
    )


def turn_sin(x):
    d = x - jnp.round(x)
    e = 0.25 - jnp.abs(d)
    q = e * e
    p = SIN_COEFS[4]
    for coef in SIN_COEFS[3::-1]:
        p = coef + q * p
    return e * p


def mm(a, b):
    return jnp.dot(a.astype(BF16), b.astype(BF16), preferred_element_type=F32)


def halves(x):
    high = x.astype(BF16)
    return high, (x - high.astype(F32)).astype(BF16)


def left_three(x):
    high, low = halves(x)
    return jnp.concatenate([high.astype(F32), high.astype(F32), low.astype(F32)], 1).astype(BF16)


def pick(row, start, count):
    shape = (count, row.shape[1])
    want = start + lax.broadcasted_iota(jnp.int32, shape, 0) % OWN
    hit = lax.broadcasted_iota(jnp.int32, shape, 1) == want
    return jnp.sum(jnp.where(hit, row.astype(F32), 0.0), axis=1, keepdims=True)


def column(row):
    count = row.shape[1]
    shape = (count, count)
    hit = lax.broadcasted_iota(jnp.int32, shape, 1) == lax.broadcasted_iota(jnp.int32, shape, 0)
    return jnp.sum(jnp.where(hit, row.astype(F32), 0.0), axis=1, keepdims=True)


def pair(x, y):
    axis = x.ndim - 2
    low = lax.broadcasted_iota(jnp.int32, x.shape, axis) < OWN
    return (
        jnp.where(low, x, pltpu.roll(y, OWN, axis)),
        jnp.where(low, pltpu.roll(x, OWN, axis), y),
    )


SMALL = 11


def fast_kernel(dims, *refs):
    tokens_h, first_h, second_h, value_h, out_w_h = refs[:5]
    small_h = refs[5 : 5 + SMALL]
    inner_h, inner_back_h, twiddle_h, outer_h, outer_back_h, feats_h, out_ref = refs[
        5 + SMALL : 12 + SMALL
    ]
    tokens_v, gates_v, out_w_v = refs[12 + SMALL : 15 + SMALL]
    small_v = refs[15 + SMALL : 15 + 2 * SMALL]
    (
        norm_gain, short_weight, short_bias, embed_weight, embed_bias, inner_weight,
        inner_bias, filter_freq, filter_weight, filter_skip, output_gain,
    ) = small_v
    (
        inner_v, inner_back_v, twiddle_v, outer_v, outer_back_v, feats_v, normed_v,
        send_a, recv_a, send_b, recv_b, send_c, recv_c, second_v, send_h, recv_h,
        taps_v, spectra, embed_pad, load_sem, small_sem, a_sems, b_sems, c_sems,
        send_h_sem, recv_h_sem,
    ) = refs[15 + 2 * SMALL :]
    rows_n, cols_n, block = dims
    length = rows_n * block
    piece = block // cols_n
    row_me = lax.axis_index("row")
    col_me = lax.axis_index("col")
    MESH = pl.DeviceIdType.MESH

    loads = [
        (tokens_h, tokens_v),
        (value_h, gates_v.at[2]),
        (first_h, gates_v.at[0]),
        (second_h, gates_v.at[1]),
        (feats_h, feats_v),
        (inner_h, inner_v),
        (twiddle_h, twiddle_v),
        (outer_h, outer_v),
        (outer_back_h, outer_back_v),
        (inner_back_h, inner_back_v),
        (out_w_h, out_w_v),
    ]
    copies = [
        pltpu.make_async_copy(src, dst, load_sem.at[i]) for i, (src, dst) in enumerate(loads)
    ]
    smalls = [
        pltpu.make_async_copy(src, dst, small_sem.at[i])
        for i, (src, dst) in enumerate(zip(small_h, small_v))
    ]
    copies[0].start()
    smalls[0].start()
    copies[1].start()
    copies[2].start()

    row_peers = [lax.rem(row_me + step, rows_n) for step in range(1, rows_n)]
    col_peers = [lax.rem(col_me + step, cols_n) for step in range(1, cols_n)]
    barrier = pltpu.get_barrier_semaphore()
    for place in [(p, col_me) for p in row_peers] + [(row_me, q) for q in col_peers]:
        pl.semaphore_signal(barrier, inc=1, device_id=place, device_id_type=MESH)

    for copy in smalls[1:] + copies[3:10]:
        copy.start()

    def exchange(send, recv, sems, me, places):
        def copy_of(src, dst, place):
            return pltpu.make_async_remote_copy(
                src_ref=src,
                dst_ref=dst,
                send_sem=sems.at[0],
                recv_sem=sems.at[1],
                device_id=place,
                device_id_type=MESH,
            )

        for peer, place in places:
            copy_of(send.at[peer], recv.at[me], place).start()
        count = len(places)
        return copy_of(send.at[pl.ds(0, count)], recv.at[pl.ds(0, count)], places[0][1])

    copies[0].wait()
    smalls[0].wait()
    gain_row = norm_gain[...]
    chunk = 32
    for start in range(0, block, chunk):
        x = tokens_v[start : start + chunk, :].astype(F32)
        scale = lax.rsqrt(jnp.mean(x * x, axis=1, keepdims=True) + NORM_EPS)
        normed_v[start : start + chunk, :] = (x * scale * gain_row).astype(BF16)

    def project(branch):
        return jnp.dot(normed_v[...], gates_v[branch], preferred_element_type=F32)

    def message(gate):
        turned = gate.T
        even, odd = pair(
            turned[:, :LANES].reshape(rows_n // 2, 2 * OWN, LANES),
            turned[:, LANES:].reshape(rows_n // 2, 2 * OWN, LANES),
        )
        return jnp.stack([even, odd], axis=1).reshape(rows_n, 2 * OWN, LANES)

    copies[1].wait()
    value_part = message(project(2))
    copies[2].wait()
    first_part = message(project(0))
    send_a[...] = jnp.concatenate([value_part, first_part], axis=1).astype(BF16)
    pl.semaphore_wait(barrier, rows_n - 1 + cols_n - 1)
    wait_a = exchange(send_a, recv_a, a_sems, row_me, [(p, (p, col_me)) for p in row_peers])
    recv_a[row_me] = send_a[row_me]

    copies[3].wait()
    gate = project(1).astype(BF16).astype(F32)
    second_v[...] = gate
    send_h[0] = gate[:1]
    send_h[1] = gate[block - 1 :]
    halo = []
    for edge, peer in ((0, row_peers[-1]), (1, row_peers[0])):
        copy = pltpu.make_async_remote_copy(
            src_ref=send_h.at[edge],
            dst_ref=recv_h.at[edge],
            send_sem=send_h_sem.at[edge],
            recv_sem=recv_h_sem.at[edge],
            device_id=(peer, col_me),
            device_id_type=MESH,
        )
        copy.start()
        halo.append(copy)
    copies[10].start()
    for copy in smalls[1:]:
        copy.wait()

    pace = filter_freq[...] * (0.5 / math.pi)
    embed_pad[...] = jnp.zeros_like(embed_pad)
    embed_pad[:FEATURES, :] = embed_weight[...] * pace
    embed_pad[FEATURES : FEATURES + 1, :] = embed_bias[...] * pace - 0.25
    embed_left = left_three(embed_pad[...].T)
    inner_left = left_three((inner_weight[...] * pace).T)
    inner_turn = column(inner_bias[...] * pace - 0.25)
    last = jnp.concatenate([filter_weight[o, d] for o in range(2) for d in range(2)], axis=1)
    last_left = left_three(last.T)
    channels = rows_n * cols_n * OWN
    slowest = math.log(DECAY_TARGET) / SLOW_SPAN
    fastest = math.log(DECAY_TARGET) / FAST_SPAN
    sub = lax.broadcasted_iota(jnp.int32, (2 * OWN, 1), 0)
    channel = ((col_me * rows_n + row_me) * OWN + sub % OWN).astype(F32)
    decay = jnp.abs(slowest + channel * ((fastest - slowest) / (channels - 1)))
    copies[4].wait()
    step_width = 1024
    for start in range(0, length, step_width):
        high = feats_v[:FEATURE_ROWS, start : start + step_width]
        low = feats_v[FEATURE_ROWS:, start : start + step_width]
        hidden = turn_sin(
            jnp.dot(
                embed_left,
                jnp.concatenate([high, low, high], 0),
                preferred_element_type=F32,
            )
        )
        high, low = halves(hidden)
        hidden = turn_sin(
            jnp.dot(
                inner_left,
                jnp.concatenate([high, low, high], 0),
                preferred_element_type=F32,
            )
            + inner_turn
        )
        high, low = halves(hidden)
        taps = jnp.dot(
            last_left, jnp.concatenate([high, low, high], 0), preferred_element_type=F32
        )
        lag = start + lax.broadcasted_iota(jnp.int32, (2 * OWN, step_width), 1)
        window = jnp.exp(-(lag.astype(F32) * (1.0 / (length - 1))) * decay)
        if start == 0:
            window = jnp.where((lag == 0) & (sub >= OWN), 0.0, window)
        for order in range(2):
            x = taps[order * 2 * OWN : (order + 1) * 2 * OWN] * window
            y = pltpu.roll(x, OWN, 0)
            x = jnp.where(sub < OWN, x + y, y - x)
            for m in range(step_width // (2 * LANES)):
                at = 2 * m * LANES
                plus, minus = pair(x[:, at : at + LANES], x[:, at + LANES : at + 2 * LANES])
                spot = (start // (2 * LANES) + m) * 2 * OWN
                lane = 2 * order * LANES
                taps_v[spot : spot + 2 * OWN, lane : lane + LANES] = plus
                taps_v[spot : spot + 2 * OWN, lane + LANES : lane + 2 * LANES] = minus

    for copy in copies[5:8]:
        copy.wait()
    depth = 2 * OWN * rows_n

    def twist(real, imag, sign):
        cos = twiddle_v[0]
        sin = twiddle_v[1] * sign
        return real * cos + imag * sin, imag * cos - real * sin

    part = mm(inner_v[...], taps_v[...])
    for order in range(2):
        for half in range(2):
            lane = (2 * order + half) * LANES
            real, imag = twist(
                part[:depth, lane : lane + LANES], part[depth:, lane : lane + LANES], 1.0
            )
            spot = slice(half * LANES, (half + 1) * LANES)
            spectra[order, :, spot] = mm(
                jnp.concatenate([real, imag], axis=1), outer_v[:, spot]
            )

    shape = (rows_n, 2 * OWN, LANES)
    low_half = lax.broadcasted_iota(jnp.int32, shape, 1) < OWN
    spot = lax.broadcasted_iota(jnp.int32, shape, 2)
    gap = jnp.zeros((1, 2 * OWN, LANES), F32)

    def smooth(x, branch):
        before = pltpu.roll(x, 1, 2)
        other = pltpu.roll(before, OWN, 1)
        earlier = jnp.concatenate([gap, other[:-1]], 0)
        before = jnp.where(spot == 0, jnp.where(low_half, earlier, other), before)
        after = pltpu.roll(x, LANES - 1, 2)
        other = pltpu.roll(after, OWN, 1)
        later = jnp.concatenate([other[1:], gap], 0)
        after = jnp.where(spot == LANES - 1, jnp.where(low_half, other, later), after)
        w = [pick(short_weight[branch, j : j + 1, :], row_me * OWN, 2 * OWN) for j in range(3)]
        bias = pick(short_bias[branch : branch + 1, :], row_me * OWN, 2 * OWN)
        return bias + before * w[0] + x * w[1] + after * w[2]

    for copy in copies[8:10]:
        copy.wait()
    skips = [pick(filter_skip[order : order + 1, :], 0, 2 * OWN) for order in range(2)]

    def convolve(signal, order):
        part = mm(inner_v[...], signal.reshape(depth, LANES))
        real, imag = twist(part[:depth], part[depth:], 1.0)
        spec = mm(jnp.concatenate([real, imag], axis=1), outer_v[...])
        sr, si = spec[:, :LANES], spec[:, LANES:]
        hr, hi = spectra[order, :, :LANES], spectra[order, :, LANES:]
        prod = jnp.concatenate([sr * hr - si * hi, sr * hi + si * hr], axis=1)
        back = mm(prod, outer_back_v[...])
        real, imag = twist(back[:, :LANES], back[:, LANES:], -1.0)
        conv = mm(inner_back_v[...], jnp.concatenate([real, imag], axis=0))
        return conv.reshape(shape) + signal * skips[order]

    wait_a.wait_recv()
    arrived = recv_a[...].astype(F32)
    signal = smooth(arrived[:, : 2 * OWN], 2)
    signal = smooth(arrived[:, 2 * OWN :], 0) * convolve(signal, 0)
    send_b[...] = convolve(signal, 1).astype(BF16)
    wait_b = exchange(send_b, recv_b, b_sems, row_me, [(p, (p, col_me)) for p in row_peers])
    recv_b[row_me] = send_b[row_me]

    for copy in halo:
        copy.wait_recv()
    x = second_v[...]
    pos = lax.broadcasted_iota(jnp.int32, x.shape, 0)
    head = jnp.where(row_me == 0, 0.0, recv_h[1])
    tail = jnp.where(row_me == rows_n - 1, 0.0, recv_h[0])
    before = jnp.where(pos == 0, head, pltpu.roll(x, 1, 0))
    after = jnp.where(pos == block - 1, tail, pltpu.roll(x, block - 1, 0))
    w = [short_weight[1, j : j + 1, :].astype(F32) for j in range(3)]
    second_v[...] = short_bias[1:2, :] + before * w[0] + x * w[1] + after * w[2]

    wait_b.wait_recv()
    x = recv_b[...].astype(F32).reshape(rows_n // 2, 2, 2 * OWN, LANES)
    early, late = pair(x[:, 0], x[:, 1])
    for j, half in enumerate((early, late)):
        at = slice(j * LANES, (j + 1) * LANES)
        x = half.reshape(LANES, LANES).T * second_v[at, :]
        scale = lax.rsqrt(jnp.mean(x * x, axis=1, keepdims=True) + NORM_EPS)
        x = x * scale * output_gain[...]
        count = LANES // piece
        send_c[j * count : (j + 1) * count] = x.astype(BF16).reshape(count, piece, LANES)
    wait_c = exchange(send_c, recv_c, c_sems, col_me, [(q, (row_me, q)) for q in col_peers])
    recv_c[col_me] = send_c[col_me]
    copies[10].wait()
    wait_c.wait_recv()
    mixed = jnp.concatenate([recv_c[q] for q in range(cols_n)], axis=1)
    step_width = 512
    for start in range(0, out_ref.shape[1], step_width):
        out_ref[:, start : start + step_width] = jnp.dot(
            mixed, out_w_v[:, start : start + step_width], preferred_element_type=F32
        ).astype(BF16)

    for copy in halo + [wait_a, wait_b, wait_c]:
        copy.wait_send()


def local(
    tokens, norm_gain, first_gate, second_gate, value_weight, short_weight, short_bias,
    embed_weight, embed_bias, inner_weight, inner_bias, filter_freq, filter_weight,
    filter_skip, output_gain, output_weight,
):
    rows_n, cols_n = lax.axis_size("row"), lax.axis_size("col")
    block, model = tokens.shape
    piece = block // cols_n
    length = block * rows_n
    width = first_gate.shape[1]
    tables = fast_tables(length)
    out_width = output_weight.shape[1]
    vm = pl.BlockSpec(memory_space=pltpu.VMEM)
    hbm = pl.BlockSpec(memory_space=pl.ANY)
    small = [
        norm_gain.reshape(1, -1),
        short_weight,
        short_bias,
        embed_weight,
        embed_bias.reshape(1, -1),
        inner_weight,
        inner_bias.reshape(1, -1),
        filter_freq.reshape(1, -1),
        filter_weight,
        filter_skip,
        output_gain.reshape(1, -1),
    ]
    operands = [tokens, first_gate, second_gate, value_weight, output_weight, *small, *tables]
    rows_all = 2 * OWN * rows_n
    DMA = pltpu.SemaphoreType.DMA
    return pl.pallas_call(
        functools.partial(fast_kernel, (rows_n, cols_n, block)),
        out_shape=pltpu.VMEM((piece, out_width), BF16),
        in_specs=[hbm] * len(operands),
        out_specs=vm,
        scratch_shapes=[
            pltpu.VMEM(tokens.shape, BF16),
            pltpu.VMEM((3, model, width), BF16),
            pltpu.VMEM(output_weight.shape, BF16),
        ]
        + [pltpu.VMEM(array.shape, array.dtype) for array in small + list(tables)]
        + [
            pltpu.VMEM(tokens.shape, BF16),
            pltpu.VMEM((rows_n, 4 * OWN, LANES), BF16),
            pltpu.VMEM((rows_n, 4 * OWN, LANES), BF16),
            pltpu.VMEM((rows_n, 2 * OWN, LANES), BF16),
            pltpu.VMEM((rows_n, 2 * OWN, LANES), BF16),
            pltpu.VMEM((cols_n, piece, LANES), BF16),
            pltpu.VMEM((cols_n, piece, LANES), BF16),
            pltpu.VMEM((block, width), F32),
            pltpu.VMEM((2, 1, width), F32),
            pltpu.VMEM((2, 1, width), F32),
            pltpu.VMEM((rows_all, 4 * LANES), F32),
            pltpu.VMEM((2, rows_all, 2 * LANES), F32),
            pltpu.VMEM((FEATURE_ROWS, embed_weight.shape[1]), F32),
            DMA((11,)),
            DMA((SMALL,)),
            DMA((2,)),
            DMA((2,)),
            DMA((2,)),
            DMA((2,)),
            DMA((2,)),
        ],
        compiler_params=pltpu.CompilerParams(
            collective_id=0, has_side_effects=True, vmem_limit_bytes=56 * 1024 * 1024
        ),
    )(*operands)


def solution(mesh):
    in_specs = (
        P("row", None),
        P(),
        P(None, "col"),
        P(None, "col"),
        P(None, "col"),
        P(None, None, "col"),
        P(None, "col"),
        P(),
        P(),
        P(),
        P(),
        P(),
        P(None, None, None, ("col", "row")),
        P(None, ("col", "row")),
        P("col"),
        P(),
    )
    out_specs = P(("row", "col"), None)
    return jax.shard_map(local, mesh=mesh, in_specs=in_specs, out_specs=out_specs, check_vma=False)
```

time: 218 us -> 34.1 us (0.16); the launches traced: 214 us -> 34 us
  local copies, waits for them, and re-layouts: 75.2 us -> 2.13 us
  matrix products: 67.1 us -> 0 us
  Pallas kernels: 0 us -> 31.8 us
  starting transfers between devices: 31.1 us -> 0 us
  blocking collectives: 30.7 us -> 0 us
  other arithmetic: 8.72 us -> 0 us
    dot_general x46 -> x0, matrix products: 67.1 us -> none  [the longest x2 13.7 us: channel_taps(): jnp.dot(hidden, filter_weight[order_index, 0], precision=HIGHEST) * window]
    pallas_call x0 -> x1, Pallas kernels: none -> 31.8 us  [local(): pl.pallas_call(functools.partial(fast_kernel, (rows_n, cols_n, block)), o...]
    all_to_all x3 -> x0, starting transfers between devices: 31.1 us -> none  [the longest x1 12 us: general_local(): lax.all_to_all(gate_value, 'row', split_axis=1, concat_axis=0, tiled=True)]
    all_to_all x2 -> x0, blocking collectives: 30.7 us -> none  [the longest x1 17.8 us: general_local(): lax.all_to_all(for_sending(signal), 'row', split_axis=0, concat_axis=1, t...]
    reshape x4 -> x0, local copies, waits for them, and re-layouts: 26.6 us -> none  [the longest x2 16.7 us: forward_taps(): flattened = circular_taps.reshape(major_size, minor_size * channels)]
    div x4 -> x0, local copies, waits for them, and re-layouts: 17 us -> none  [inverse(): values.reshape(half_rows * minor_size, channels) / (major_size * minor_size)]
    concatenate x4 -> x0, local copies, waits for them, and re-layouts: 10.7 us -> none  [two_sided(): jnp.concatenate([forward, jnp.zeros_like(forward[:1]), backward[:0:-1]],...]
    unnamed x42 -> x2, local copies, waits for them, and re-layouts: 11.5 us -> 2.13 us
  transfers between devices with their start and end apart: 3 -> 0, of which waited for: 0 -> 0; matrix products, arithmetic and copies ran while one was open for 66% -> 0% of each run, Pallas kernels for 0% -> 0%
where the time goes in v1:
time: 34.1 us; the launch traced here: 34 us
  Pallas kernels  31.8 us (93%)
  local copies, waits for them, and re-layouts  2.13 us (6%)
    pallas_call x1, Pallas kernels, local(): pl.pallas_call(functools.partial(fast_kernel, (rows_n, cols_n, block)), o...  31.8 us
    unnamed x2, local copies, waits for them, and re-layouts  2.13 us

profile of v1, /device:TPU:1, one launch (start us, length us, event | category | flops | bytes accessed | tf_op | source)
XLA Modules:
  0.0 34.0 jit_solution(6544396558054706293)
XLA Ops:
  0.0 1.5 %copy.23.refs_13_ = f32[2,2,64,4]{3,2,1,0:T(8,128)} copy(f32[2,2,64,4]{2,3,1,0:T(4,128)} %param.34) | data formatting | bytes 8192 | tf_op args[12]
  1.5 31.8 %shard_map.208 = bf16[32,2048]{1,0:T(8,128)(2,1)S(1)} custom-call(bf16[256,2048]{1,0:T(8,128)(2,1)} %refs_0_.1, bf16[2048,128]{1,0:T(8,128)(2,1)} %refs_1_.1, bf16[2048,128]{1,0:T(8,128)(2,1)} %refs_2_.1, bf16[2048,128]{1,0:T(8,128)(2,1)} %refs_3_.1, bf16[1024,2048]{1,0:T(8,128)(2,1)} %refs_4_.1, f32[1,2048]{1,0:T(1,128)} %bitcast.5, ...), custom_call_target="tpu_custom_call" | custom-call | tf_op jit(solution)/shard_map/pallas_call | solution.py:428
  33.3 0.7 %copy.25 = bf16[32,2048]{1,0:T(8,128)(2,1)} copy(bf16[32,2048]{1,0:T(8,128)(2,1)S(1)} %shard_map.208) | data formatting | bytes 262144

commit v2 on v1

--- a/solution.py
+++ b/solution.py
@@ -18,6 +18,7 @@
 SLOW_SPAN = 1.5
 LANES = 128
 OWN = 4
+EARLY_WIDTH = 1024
 FEATURE_ROWS = 48
 BF16 = jnp.bfloat16
 F32 = jnp.float32
@@ -113,6 +114,17 @@
 
 
 SMALL = 11
+ROW_MINOR = 4
+COL_MINOR = 2
+
+
+def far_first(me, count, minor):
+    major = count // minor
+    majors = [lax.rem(lax.div(me, minor) + d, major) * minor for d in range(major)]
+    minors = [lax.rem(lax.rem(me, minor) + d, minor) for d in range(minor)]
+    offsets = [(a, b) for a in range(major) for b in range(minor) if a or b]
+    offsets.sort(key=lambda o: -(min(o[0], major - o[0]) + min(o[1], minor - o[1])))
+    return [majors[a] + minors[b] for a, b in offsets]
 
 
 def fast_kernel(dims, *refs):
@@ -160,17 +172,21 @@
         pltpu.make_async_copy(src, dst, small_sem.at[i])
         for i, (src, dst) in enumerate(zip(small_h, small_v))
     ]
+    row_peers = far_first(row_me, rows_n, ROW_MINOR)
+    col_peers = far_first(col_me, cols_n, COL_MINOR)
+    barrier = pltpu.get_barrier_semaphore()
+    places = [(p, col_me) for p in row_peers] + [(row_me, q) for q in col_peers]
+
+    def greet(some):
+        for place in some:
+            pl.semaphore_signal(barrier, inc=1, device_id=place, device_id_type=MESH)
+
+    greet(places[:8])
     copies[0].start()
     smalls[0].start()
     copies[1].start()
     copies[2].start()
-
-    row_peers = [lax.rem(row_me + step, rows_n) for step in range(1, rows_n)]
-    col_peers = [lax.rem(col_me + step, cols_n) for step in range(1, cols_n)]
-    barrier = pltpu.get_barrier_semaphore()
-    for place in [(p, col_me) for p in row_peers] + [(row_me, q) for q in col_peers]:
-        pl.semaphore_signal(barrier, inc=1, device_id=place, device_id_type=MESH)
-
+    greet(places[8:])
     for copy in smalls[1:] + copies[3:10]:
         copy.start()
 
@@ -211,32 +227,12 @@
         return jnp.stack([even, odd], axis=1).reshape(rows_n, 2 * OWN, LANES)
 
     copies[1].wait()
-    value_part = message(project(2))
+    send_a[0] = message(project(2)).astype(BF16)
     copies[2].wait()
-    first_part = message(project(0))
-    send_a[...] = jnp.concatenate([value_part, first_part], axis=1).astype(BF16)
-    pl.semaphore_wait(barrier, rows_n - 1 + cols_n - 1)
-    wait_a = exchange(send_a, recv_a, a_sems, row_me, [(p, (p, col_me)) for p in row_peers])
-    recv_a[row_me] = send_a[row_me]
-
-    copies[3].wait()
-    gate = project(1).astype(BF16).astype(F32)
-    second_v[...] = gate
-    send_h[0] = gate[:1]
-    send_h[1] = gate[block - 1 :]
-    halo = []
-    for edge, peer in ((0, row_peers[-1]), (1, row_peers[0])):
-        copy = pltpu.make_async_remote_copy(
-            src_ref=send_h.at[edge],
-            dst_ref=recv_h.at[edge],
-            send_sem=send_h_sem.at[edge],
-            recv_sem=recv_h_sem.at[edge],
-            device_id=(peer, col_me),
-            device_id_type=MESH,
-        )
-        copy.start()
-        halo.append(copy)
-    copies[10].start()
+    send_a[1] = message(project(0)).astype(BF16)
+    recv_a[0, row_me] = send_a[0, row_me]
+    recv_a[1, row_me] = send_a[1, row_me]
+
     for copy in smalls[1:]:
         copy.wait()
 
@@ -247,8 +243,8 @@
     embed_left = left_three(embed_pad[...].T)
     inner_left = left_three((inner_weight[...] * pace).T)
     inner_turn = column(inner_bias[...] * pace - 0.25)
-    last = jnp.concatenate([filter_weight[o, d] for o in range(2) for d in range(2)], axis=1)
-    last_left = left_three(last.T)
+    last = jnp.concatenate([filter_weight[o, d] for o in range(2) for d in range(2)], axis=0)
+    last_left = left_three(last)
     channels = rows_n * cols_n * OWN
     slowest = math.log(DECAY_TARGET) / SLOW_SPAN
     fastest = math.log(DECAY_TARGET) / FAST_SPAN
@@ -256,10 +252,9 @@
     channel = ((col_me * rows_n + row_me) * OWN + sub % OWN).astype(F32)
     decay = jnp.abs(slowest + channel * ((fastest - slowest) / (channels - 1)))
     copies[4].wait()
-    step_width = 1024
-    for start in range(0, length, step_width):
-        high = feats_v[:FEATURE_ROWS, start : start + step_width]
-        low = feats_v[FEATURE_ROWS:, start : start + step_width]
+    def filter_part(start, width):
+        high = feats_v[:FEATURE_ROWS, start : start + width]
+        low = feats_v[FEATURE_ROWS:, start : start + width]
         hidden = turn_sin(
             jnp.dot(
                 embed_left,
@@ -280,7 +275,7 @@
         taps = jnp.dot(
             last_left, jnp.concatenate([high, low, high], 0), preferred_element_type=F32
         )
-        lag = start + lax.broadcasted_iota(jnp.int32, (2 * OWN, step_width), 1)
+        lag = start + lax.broadcasted_iota(jnp.int32, (2 * OWN, width), 1)
         window = jnp.exp(-(lag.astype(F32) * (1.0 / (length - 1))) * decay)
         if start == 0:
             window = jnp.where((lag == 0) & (sub >= OWN), 0.0, window)
@@ -288,7 +283,7 @@
             x = taps[order * 2 * OWN : (order + 1) * 2 * OWN] * window
             y = pltpu.roll(x, OWN, 0)
             x = jnp.where(sub < OWN, x + y, y - x)
-            for m in range(step_width // (2 * LANES)):
+            for m in range(width // (2 * LANES)):
                 at = 2 * m * LANES
                 plus, minus = pair(x[:, at : at + LANES], x[:, at + LANES : at + 2 * LANES])
                 spot = (start // (2 * LANES) + m) * 2 * OWN
@@ -296,6 +291,33 @@
                 taps_v[spot : spot + 2 * OWN, lane : lane + LANES] = plus
                 taps_v[spot : spot + 2 * OWN, lane + LANES : lane + 2 * LANES] = minus
 
+
+    filter_part(0, EARLY_WIDTH)
+    pl.semaphore_wait(barrier, rows_n - 1 + cols_n - 1)
+    row_places = [(p, (p, col_me)) for p in row_peers]
+    wait_a = [
+        exchange(send_a.at[i], recv_a.at[i], a_sems.at[i], row_me, row_places) for i in range(2)
+    ]
+    copies[3].wait()
+    gate = project(1).astype(BF16).astype(F32)
+    second_v[...] = gate
+    send_h[0] = gate[:1]
+    send_h[1] = gate[block - 1 :]
+    halo = []
+    for edge, shift in ((0, rows_n - 1), (1, 1)):
+        peer = lax.rem(row_me + shift, rows_n)
+        copy = pltpu.make_async_remote_copy(
+            src_ref=send_h.at[edge],
+            dst_ref=recv_h.at[edge],
+            send_sem=send_h_sem.at[edge],
+            recv_sem=recv_h_sem.at[edge],
+            device_id=(peer, col_me),
+            device_id_type=MESH,
+        )
+        copy.start()
+        halo.append(copy)
+    copies[10].start()
+    filter_part(EARLY_WIDTH, length - EARLY_WIDTH)
     for copy in copies[5:8]:
         copy.wait()
     depth = 2 * OWN * rows_n
@@ -351,12 +373,12 @@
         conv = mm(inner_back_v[...], jnp.concatenate([real, imag], axis=0))
         return conv.reshape(shape) + signal * skips[order]
 
-    wait_a.wait_recv()
-    arrived = recv_a[...].astype(F32)
-    signal = smooth(arrived[:, : 2 * OWN], 2)
-    signal = smooth(arrived[:, 2 * OWN :], 0) * convolve(signal, 0)
+    wait_a[0].wait_recv()
+    signal = convolve(smooth(recv_a[0].astype(F32), 2), 0)
+    wait_a[1].wait_recv()
+    signal = smooth(recv_a[1].astype(F32), 0) * signal
     send_b[...] = convolve(signal, 1).astype(BF16)
-    wait_b = exchange(send_b, recv_b, b_sems, row_me, [(p, (p, col_me)) for p in row_peers])
+    wait_b = exchange(send_b, recv_b, b_sems, row_me, row_places)
     recv_b[row_me] = send_b[row_me]
 
     for copy in halo:
@@ -391,7 +413,7 @@
             mixed, out_w_v[:, start : start + step_width], preferred_element_type=F32
         ).astype(BF16)
 
-    for copy in halo + [wait_a, wait_b, wait_c]:
+    for copy in halo + wait_a + [wait_b, wait_c]:
         copy.wait_send()
 
 
@@ -418,7 +440,7 @@
         inner_weight,
         inner_bias.reshape(1, -1),
         filter_freq.reshape(1, -1),
-        filter_weight,
+        jnp.swapaxes(filter_weight, 2, 3),
         filter_skip,
         output_gain.reshape(1, -1),
     ]
@@ -438,8 +460,8 @@
         + [pltpu.VMEM(array.shape, array.dtype) for array in small + list(tables)]
         + [
             pltpu.VMEM(tokens.shape, BF16),
-            pltpu.VMEM((rows_n, 4 * OWN, LANES), BF16),
-            pltpu.VMEM((rows_n, 4 * OWN, LANES), BF16),
+            pltpu.VMEM((2, rows_n, 2 * OWN, LANES), BF16),
+            pltpu.VMEM((2, rows_n, 2 * OWN, LANES), BF16),
             pltpu.VMEM((rows_n, 2 * OWN, LANES), BF16),
             pltpu.VMEM((rows_n, 2 * OWN, LANES), BF16),
             pltpu.VMEM((cols_n, piece, LANES), BF16),
@@ -452,7 +474,7 @@
             pltpu.VMEM((FEATURE_ROWS, embed_weight.shape[1]), F32),
             DMA((11,)),
             DMA((SMALL,)),
-            DMA((2,)),
+            DMA((2, 2)),
             DMA((2,)),
             DMA((2,)),
             DMA((2,)),

time: 34.1 us -> 30.7 us (0.900)
  Pallas kernels: 31.8 us -> 29.9 us
  local copies, waits for them, and re-layouts: 2.13 us -> 0.66 us
    pallas_call x1, Pallas kernels: 31.8 us -> 29.9 us  [local(): pl.pallas_call(functools.partial(fast_kernel, (rows_n, cols_n, block)), o...]
    unnamed x2 -> x1, local copies, waits for them, and re-layouts: 2.13 us -> 0.66 us
where the time goes in v2:
time: 30.7 us; the launch traced here: 30.6 us
  Pallas kernels  29.9 us (97%)
  local copies, waits for them, and re-layouts  0.66 us (2%)
    pallas_call x1, Pallas kernels, local(): pl.pallas_call(functools.partial(fast_kernel, (rows_n, cols_n, block)), o...  29.9 us
    unnamed x1, local copies, waits for them, and re-layouts  0.66 us

profile of v2, /device:TPU:1, one launch (start us, length us, event | category | flops | bytes accessed | tf_op | source)
XLA Modules:
  0.0 30.6 jit_solution(18077735461679788051)
XLA Ops:
  0.0 29.9 %shard_map.208 = bf16[32,2048]{1,0:T(8,128)(2,1)S(1)} custom-call(bf16[256,2048]{1,0:T(8,128)(2,1)} %refs_0_.1, bf16[2048,128]{1,0:T(8,128)(2,1)} %refs_1_.1, bf16[2048,128]{1,0:T(8,128)(2,1)} %refs_2_.1, bf16[2048,128]{1,0:T(8,128)(2,1)} %refs_3_.1, bf16[1024,2048]{1,0:T(8,128)(2,1)} %refs_4_.1, f32[1,2048]{1,0:T(1,128)} %bitcast.6, ...), custom_call_target="tpu_custom_call" | custom-call | tf_op jit(solution)/shard_map/pallas_call | solution.py:450
  29.9 0.7 %copy.24 = bf16[32,2048]{1,0:T(8,128)(2,1)} copy(bf16[32,2048]{1,0:T(8,128)(2,1)S(1)} %shard_map.208) | data formatting | bytes 262144
